TPU v7x, 32 devices: a whole 2x2x4 slice. The times are simulated.
32 devices in a mesh: sp: 4 (over z), fs: 4 (over y, x), tp: 2 (over core).
Axes of the slice: x: 2, y: 2, z: 4, core: 2. Of those that a mesh axis runs over, the one named last changes fastest.
Arguments:
- tokens: bfloat16 [4, 1024, 2048], P('fs', 'sp', 'tp'), may hold values from -6 to 6
- norm_gain: float32 [2048], replicated, may hold values from 0.1 to 1.9
- ret_query: bfloat16 [2048, 1024], P('sp', 'tp'), may hold values from -0.125 to 0.125
- ret_key: bfloat16 [2048, 1024], P('sp', 'tp'), may hold values from -0.125 to 0.125
- ret_value: bfloat16 [2048, 1024], P('sp', 'tp'), may hold values from -0.125 to 0.125
- att_query: bfloat16 [2048, 1024], P('sp', 'tp'), may hold values from -0.125 to 0.125
- att_key: bfloat16 [2048, 256], P('sp', 'tp'), may hold values from -0.125 to 0.125
- att_value: bfloat16 [2048, 256], P('sp', 'tp'), may hold values from -0.125 to 0.125
- log_decay: float32 [4, 4, 1024], P('fs', 'tp', 'sp'), may hold values from -1 to 0
- start_state: float32 [4, 4, 256, 256], P('fs', 'tp'), may hold values from -12 to 12
- ret_gain: float32 [1024], P('tp'), may hold values from 0.1 to 1.9
- sink_logits: float32 [16], P('tp'), may hold values from 1 to 5
- ret_out: bfloat16 [1024, 2048], P('tp', 'fs'), may hold values from -0.1875 to 0.1875
- att_out: bfloat16 [1024, 2048], P('tp', 'fs'), may hold values from -1.5 to 1.5
Outputs:
- mixed: bfloat16 [4, 1024, 2048], P('fs', 'sp', 'tp')
All inputs are finite; a program needn't handle non-finite values.
Results may differ from a plain program's by a relative error of at most 0.015.
Values may be sent and summed in bfloat16 or wider, within the bound.
A program may use at most 128 MiB of HBM per device.

v0:
```python
import jax
import jax.numpy as jnp
from jax import lax
from jax.sharding import PartitionSpec as P

DK = 256
DV = 256
HD = 64
WINDOW = 128
BLOCK = 128
epsilon = 1e-06
exact_result = lax.Precision.HIGHEST


def carried_in(array, axis, combine, identity):
    peers, mine = (lax.axis_size(axis), lax.axis_index(axis))
    everything = jax.tree.map(
        lambda part, kind: lax.all_gather(part.astype(kind), axis),
        array,
        (jnp.bfloat16, jnp.bfloat16),
    )
    start = jax.tree.map(
        lambda part, zero: jnp.broadcast_to(jnp.asarray(zero, part.dtype), part.shape),
        array,
        identity,
    )

    def hop(k, before):
        reached = k < mine
        new = combine(
            before, jax.tree.map(lambda part, own: part[k].astype(own.dtype), everything, array)
        )
        return jax.tree.map(lambda a, b: jnp.where(reached, a, b), new, before)

    return lax.fori_loop(0, peers, hop, start)


def passed_along(block, axis, distance):
    devices = range(lax.axis_size(axis))
    route = [(i - distance, i) for i in devices if i - distance in devices]
    return lax.ppermute(block, axis, route)


def rotate(values, positions):
    half_dim = values.shape[-1] // 2
    inverse = 1.0 / 10000.0 ** (jnp.arange(half_dim, dtype=jnp.float32) / half_dim)
    angles = positions.astype(jnp.float32)[:, None] * inverse[None, :]
    cosine = jnp.cos(angles)[:, None, :]
    sine_table = jnp.sin(angles)[:, None, :]
    front_half = values[..., :half_dim]
    back_half = values[..., half_dim:]
    return jnp.concatenate(
        [
            front_half * cosine - back_half * sine_table,
            front_half * sine_table + back_half * cosine,
        ],
        axis=-1,
    )


def block_step(memory_state, inputs):
    queries, key_matrix_rows, value_matrix_rows, log_rates = inputs
    length_here = log_rates.shape[-1]
    causal = jnp.arange(length_here)[:, None] >= jnp.arange(length_here)[None, :]
    running_totals = jnp.cumsum(log_rates, axis=-1)
    relative = running_totals[:, :, None] - running_totals[:, None, :]
    weight = jnp.where(causal[None], jnp.exp(jnp.where(causal[None], relative, 0.0)), 0.0)
    score_matrix = (
        jnp.einsum("hqd,hkd->hqk", queries, key_matrix_rows, precision=exact_result) * weight
    )
    carried_state = jnp.einsum(
        "hqd,hdv->hqv",
        queries * jnp.exp(running_totals)[:, :, None],
        memory_state,
        precision=exact_result,
    )
    output_rows = (
        jnp.einsum("arf,afu->aru", score_matrix, value_matrix_rows, precision=exact_result)
        + carried_state
    )
    decay_factors = jnp.exp(running_totals[:, -1:] - running_totals)
    memory_state = memory_state * jnp.exp(running_totals[:, -1])[:, None, None] + jnp.einsum(
        "iwj,iwe->ije",
        key_matrix_rows * decay_factors[:, :, None],
        value_matrix_rows,
        precision=exact_result,
    )
    return (memory_state, output_rows)


def chain(earlier, later):
    return (earlier[0] * later[0], earlier[1] * later[0][:, None, None] + later[1])


def shards(
    tokens,
    norm_gain,
    ret_query,
    ret_key,
    ret_value,
    att_query,
    att_key,
    att_value,
    log_decay,
    start_state,
    ret_gain,
    sink_logits,
    ret_out,
    att_out,
):
    gathered = lax.all_gather(tokens[0], "tp", axis=1, tiled=True)
    row_count = gathered.shape[0]
    as_float = gathered.astype(jnp.float32)
    normed = (
        as_float
        * lax.rsqrt(jnp.mean(as_float * as_float, axis=-1, keepdims=True) + epsilon)
        * norm_gain
    ).astype(jnp.bfloat16)
    offset = lax.axis_index("sp") * row_count
    positions = offset + jnp.arange(row_count, dtype=jnp.int32)
    weights = (ret_query, ret_key, ret_value, att_query, att_key, att_value)
    pieces = (
        lax.all_gather(weights[0], "sp", axis=0, tiled=True),
        lax.all_gather(weights[1], "sp", axis=0, tiled=True),
        lax.all_gather(weights[2], "sp", axis=0, tiled=True),
        lax.all_gather(weights[3], "sp", axis=0, tiled=True),
        lax.all_gather(weights[4], "sp", axis=0, tiled=True),
        lax.all_gather(weights[5], "sp", axis=0, tiled=True),
    )
    projected = tuple(
        (jnp.dot(normed, piece, preferred_element_type=jnp.float32) for piece in pieces)
    )
    rounded = tuple((product_f.astype(jnp.bfloat16) for product_f in projected))
    projected = rounded[:3]
    head_count = projected[0].shape[1] // DK
    queries = rotate(projected[0].astype(jnp.float32).reshape(row_count, head_count, DK), positions)
    keys_rot = rotate(
        projected[1].astype(jnp.float32).reshape(row_count, head_count, DK), positions
    ) * DK ** (-0.5)
    values_f = projected[2].astype(jnp.float32).reshape(row_count, head_count, DV)
    log_rates = log_decay[0]
    count = row_count // BLOCK

    def blocked(array):
        return array.reshape(count, BLOCK, head_count, array.shape[-1]).transpose(0, 2, 1, 3)

    rates_blocked = log_rates.reshape(head_count, count, BLOCK).transpose(1, 0, 2)
    local_state, pieces = lax.scan(
        block_step,
        jnp.zeros((head_count, DK, DV), jnp.float32),
        (blocked(queries), blocked(keys_rot), blocked(values_f), rates_blocked),
    )
    local_out = pieces.transpose(0, 2, 1, 3).reshape(row_count, head_count, DV)
    running_totals = jnp.cumsum(log_rates, axis=-1)
    device_decay = jnp.exp(running_totals[:, -1])
    identity = (jnp.ones((head_count,), jnp.float32), jnp.zeros((head_count, DK, DV), jnp.float32))
    prior_decay, prior_state = carried_in((device_decay, local_state), "sp", chain, identity)
    incoming = prior_state + prior_decay[:, None, None] * start_state[0]
    retained = local_out + jnp.einsum(
        "thd,hdv->thv",
        queries * jnp.exp(running_totals).T[:, :, None],
        incoming,
        precision=exact_result,
    )
    centred = retained - jnp.mean(retained, axis=-1, keepdims=True)
    variance = jnp.mean(centred * centred, axis=-1, keepdims=True)
    ret_hidden = (
        (centred * lax.rsqrt(variance + epsilon)).reshape(row_count, head_count * DV) * ret_gain
    ).astype(jnp.bfloat16)
    att_queries, att_keys, att_values = rounded[3:]
    kv_heads = att_keys.shape[1] // HD
    groups = att_queries.shape[1] // HD // kv_heads
    earlier_keys, earlier_values = passed_along(
        (att_keys[row_count - WINDOW :], att_values[row_count - WINDOW :]), "sp", 1
    )
    extended_keys = jnp.concatenate([earlier_keys, att_keys], axis=0)
    extended_values = jnp.concatenate([earlier_values, att_values], axis=0)
    windows = row_count // WINDOW

    def banded(array):
        earlier = array[:row_count].reshape(windows, WINDOW, kv_heads, HD)
        current = array[WINDOW:].reshape(windows, WINDOW, kv_heads, HD)
        return jnp.concatenate([earlier, current], axis=1)

    key_band = banded(extended_keys)
    value_band = banded(extended_values)
    grouped_q = att_queries.reshape(windows, WINDOW, kv_heads, groups, HD)
    score_matrix = jnp.einsum(
        "nqhgd,nkhd->nhgqk", grouped_q, key_band, preferred_element_type=jnp.float32
    ) * HD ** (-0.5)
    query_index = WINDOW + jnp.arange(WINDOW)
    key_index = jnp.arange(2 * WINDOW)
    allowed = (key_index[None, :] <= query_index[:, None]) & (
        query_index[:, None] - key_index[None, :] < WINDOW
    )
    key_place = offset - WINDOW + jnp.arange(windows)[:, None] * WINDOW + key_index[None, :]
    visible = (allowed[None] & (key_place >= 0)[:, None, :])[:, None, None]
    expo = jnp.exp(jnp.where(visible, score_matrix, -1e30))
    summed = jnp.sum(expo, axis=-1, keepdims=True) + jnp.exp(sink_logits).reshape(
        1, kv_heads, groups, 1, 1
    )
    probs = (expo / summed).astype(jnp.bfloat16)
    attended = jnp.einsum(
        "nhgqk,nkhd->nqhgd", probs, value_band, preferred_element_type=jnp.float32
    )
    att_hidden = attended.astype(jnp.bfloat16).reshape(row_count, kv_heads * groups * HD)
    ret_width = ret_hidden.shape[1]
    joined = jnp.concatenate([ret_hidden, att_hidden], axis=1)[None]
    piece = lax.all_gather(joined, "fs", axis=0, tiled=True)
    product = jnp.einsum(
        "srh,hd->srd", piece[:, :, :ret_width], ret_out, preferred_element_type=jnp.float32
    )
    product = product + jnp.einsum(
        "srh,hd->srd", piece[:, :, ret_width:], att_out, preferred_element_type=jnp.float32
    )
    partial_rows = product.astype(jnp.bfloat16)
    regrouped = lax.all_to_all(partial_rows, "fs", split_axis=0, concat_axis=2, tiled=True)
    mixed = lax.psum_scatter(
        regrouped[0].astype(jnp.float32).astype(jnp.bfloat16), "tp", scatter_dimension=1, tiled=True
    )
    return mixed[None]


def solution(mesh):
    placed = (
        P("fs", "sp", "tp"),
        P(),
        P("sp", "tp"),
        P("sp", "tp"),
        P("sp", "tp"),
        P("sp", "tp"),
        P("sp", "tp"),
        P("sp", "tp"),
        P("fs", "tp", "sp"),
        P("fs", "tp", None, None),
        P("tp"),
        P("tp"),
        P("tp", "fs"),
        P("tp", "fs"),
    )
    return jax.shard_map(
        shards, mesh=mesh, in_specs=placed, out_specs=P("fs", "sp", "tp"), check_vma=False
    )
```

profile of v0, /device:TPU:0, one launch (start us, length us, event | category | flops | bytes accessed | tf_op | source)
XLA Modules:
  0.0 330.0 jit_solution(6295431087866726067)
XLA Ops:
  6.6 0.7 all-gather.20.cloned.1.call-update
  7.3 0.7 all-gather.12.cloned.1.call-update
  8.1 0.7 all-gather.16.cloned.1.call-update
  13.0 13.6 %all-reduce = bf16[8]{0:T(256)(128)(2,1)S(1)} all-reduce(bf16[8]{0:T(256)(128)(2,1)S(1)} %dynamic-update-slice), channel_id=3, replica_groups=mesh['sp'=4,'fs'=4,'tp'=2] {'sp'}, use_global_device_ids=true, to_apply=%add | all-reduce | flops 8 | bytes 32
  26.6 18.4 %all_gather.42 = bf16[2048,128]{1,0:T(8,128)(2,1)S(1)} all-gather(bf16[512,128]{1,0:T(8,128)(2,1)S(1)} %copy-done.12), channel_id=1, replica_groups=mesh['sp'=4,'fs'=4,'tp'=2] {'sp'}, dimensions={0}, use_global_device_ids=true | all-gather | bytes 655360 | tf_op jit(solution)/shard_map/all_gather | solution.py:127
  45.7 21.2 %all_gather.41 = bf16[2048,128]{1,0:T(8,128)(2,1)} all-gather(bf16[512,128]{1,0:T(8,128)(2,1)S(1)} %copy-done.13), channel_id=1, replica_groups=mesh['sp'=4,'fs'=4,'tp'=2] {'sp'}, dimensions={0}, use_global_device_ids=true | all-gather | bytes 655360 | tf_op jit(solution)/shard_map/all_gather | solution.py:128
  66.9 1.2 multiply_cosine_fusion
  68.1 0.8 broadcast_and_fusion
  68.9 1.6 fusion.25
  70.5 1.7 convolution_convert_fusion.5
  72.9 2.6 collective-permute-start.1
  75.5 5.5 %all-gather.12.cloned.1.call-done = bf16[2048,512]{1,0:T(8,128)(2,1)} async-done(((bf16[512,512]{1,0:T(8,128)(2,1)}), bf16[2048,512]{1,0:T(8,128)(2,1)}) %all-gather.12.cloned.1.call-update) | async-done | bytes 2097168 | tf_op jit(solution)/shard_map/all_gather | solution.py:124
  80.9 2.3 fusion.31
  83.6 44.0 %all-gather.16.cloned.1.call-done = bf16[2048,512]{1,0:T(8,128)(2,1)} async-done(((bf16[512,512]{1,0:T(8,128)(2,1)}), bf16[2048,512]{1,0:T(8,128)(2,1)}) %all-gather.16.cloned.1.call-update) | async-done | bytes 2097168 | tf_op jit(solution)/shard_map/all_gather | solution.py:123
  127.6 2.7 fusion.33
  130.3 1.1 reshape.299
  131.4 42.1 %all-gather.14.cloned.1.call-done = bf16[2048,512]{1,0:T(8,128)(2,1)} async-done(((bf16[512,512]{1,0:T(8,128)(2,1)}), bf16[2048,512]{1,0:T(8,128)(2,1)}) %all-gather.14.cloned.1.call-update) | async-done | bytes 2097168 | tf_op jit(solution)/shard_map/all_gather | solution.py:125
  173.6 2.7 fusion.32
  176.6 1.3 fusion.65
  178.9 6.7 %while.29 = (s32[]{:T(128)}, f32[2,256,256]{2,1,0:T(8,128)S(1)}, f32[2,2,128,256]{3,2,1,0:T(8,128)}, f32[2,2,128]{2,1,0:T(2,128)S(1)}, f32[2,2,128,256]{3,2,0,1:...) while((s32[]{:T(128)}, f32[2,256,256]{2,1,0:T(8,128)S(1)}, ...), condition=%wide.region_3.4_spmd.clone, body=%wide.region_1.3_spmd.clone.sunk | while | flops 604880896 | bytes 4242084 | solution.py:148
  180.2 1.2 fusion.95
  181.4 0.8 convolution_add_fusion.3
  183.6 1.2 fusion.95
  184.8 0.8 convolution_add_fusion.3
  185.6 0.7 convert_element_type.102
  186.4 1.9 convolution_convert_fusion.6
  188.6 2.3 collective-permute-start
  191.0 0.8 pad_maximum_fusion.2
  192.0 1.0 collective-permute-done
  193.2 1.3 copy.65
  194.9 24.5 %all-gather.18.cloned.1.call-done = bf16[2048,512]{1,0:T(8,128)(2,1)} async-done(((bf16[512,512]{1,0:T(8,128)(2,1)}), bf16[2048,512]{1,0:T(8,128)(2,1)}) %all-gather.18.cloned.1.call-update) | async-done | bytes 2097168 | tf_op jit(solution)/shard_map/all_gather | solution.py:126
  219.5 2.3 convolution_convert_fusion.1
  223.8 25.1 %all-gather.22.cloned.1.call-done = bf16[8,256,256]{2,1,0:T(8,128)(2,1)} async-done(((bf16[2,256,256]{2,1,0:T(8,128)(2,1)}), bf16[8,256,256]{2,1,0:T(8,128)(2,1)}) %all-gather.22.cloned.1.call-update) | async-done | bytes 1048592 | tf_op jit(solution)/shard_map/all_gather | solution.py:18
  248.9 4.6 %while.30 = (s32[]{:T(128)}, f32[2]{0:T(128)S(1)}, f32[2,256,256]{2,1,0:T(8,128)S(1)}, s32[]{:T(128)}, bf16[4,2]{1,0:T(4,128)(2,1)S(1)}, /*index=5*/bf16[4,2,256,256]{3,2,1,0:T(8,128)(2,1)}, s32[]{:T(128)}, s32[]{:T(128)}) while((s32[]{:T(128)}, f32[2]{0:T(128)S(1)}, f32[2,256,256]{2,1,0:T(8,128)S(1)}, s32[]{:T(128)}, ...), condition=%wide.region_7.8_spmd.clone, body=%wide.region_6.7_spmd.clone.sunk | while | flops 655372 | bytes 1310871 | solution.py:35
  248.9 1.2 fusion.96
  250.1 1.1 fusion.96
  251.3 1.1 fusion.96
  252.4 1.1 fusion.96
  253.6 1.2 fusion.67
  255.0 0.8 pad_maximum_fusion.1
  255.9 34.5 %all-gather.24.cloned.1.call-done = bf16[1024,1024]{0,1:T(8,128)(2,1)} async-done(((bf16[256,1024]{0,1:T(8,128)(2,1)}), bf16[1024,1024]{0,1:T(8,128)(2,1)}) %all-gather.24.cloned.1.call-update) | async-done | bytes 2097168 | tf_op jit(solution)/shard_map/all_gather | solution.py:209
  290.4 2.9 copy.81
  293.3 0.7 fusion.36
  294.4 0.7 add_convert_fusion
  295.1 16.7 %all_to_all.15 = bf16[4,256,512]{2,1,0:T(8,128)(2,1)S(1)} all-to-all(bf16[4,256,512]{2,1,0:T(8,128)(2,1)S(1)} %add_convert_fusion), channel_id=1, replica_groups=mesh['sp'=4,'fs'=4,'tp'=2] {'fs'}, dimensions={0} | all-to-all | bytes 2097152 | tf_op jit(solution)/shard_map/all_to_all | solution.py:217
  311.8 1.3 copy.82
  313.1 8.0 %reduce-scatter.2.cloned.1.call-done = bf16[256,1024]{0,1:T(8,128)(2,1)} async-done(((bf16[256,2048]{0,1:T(8,128)(2,1)}), bf16[256,1024]{0,1:T(8,128)(2,1)}) %reduce-scatter.2.cloned.1.call-update) | async-done | bytes 524304 | tf_op jit(solution)/shard_map/reduce_scatter | solution.py:218
  321.1 2.0 copy.83
  (138 shorter events, 13.2 us)
Async XLA Ops:
  6.5 286.8 %copy-start = (bf16[512,512]{1,0:T(8,128)(2,1)S(1)}, bf16[512,512]{1,0:T(8,128)(2,1)}, u32[]{:S(2)}) copy-start(bf16[512,512]{1,0:T(8,128)(2,1)} %param.30) | copy-start | bytes 1572868
  6.5 4.8 %copy-start.23 = (u32[32]{0:T(128)S(1)}, u32[32]{0:T(128)}, u32[]{:S(2)}) copy-start(u32[32]{0:T(128)} %constant.93) | copy-start | bytes 388
  6.5 3.5 %copy-start.15 = (f32[1,2,256]{2,1,0:T(2,128)S(1)}, f32[1,2,256]{2,1,0:T(2,128)}, u32[]{:S(2)}) copy-start(f32[1,2,256]{2,1,0:T(2,128)} %param.26) | copy-start | bytes 6148
  6.5 20.1 %copy-start.12 = (bf16[512,128]{1,0:T(8,128)(2,1)S(1)}, bf16[512,128]{1,0:T(8,128)(2,1)}, u32[]{:S(2)}) copy-start(bf16[512,128]{1,0:T(8,128)(2,1)} %param.24) | copy-start | bytes 393220
  6.5 38.6 %copy-start.22 = (f32[8]{0:T(128)S(1)}, f32[8]{0:T(128)}, u32[]{:S(2)}) copy-start(f32[8]{0:T(128)} %param.29) | copy-start | bytes 100
  6.5 39.2 %copy-start.13 = (bf16[512,128]{1,0:T(8,128)(2,1)S(1)}, bf16[512,128]{1,0:T(8,128)(2,1)}, u32[]{:S(2)}) copy-start(bf16[512,128]{1,0:T(8,128)(2,1)} %param.25) | copy-start | bytes 393220
  6.6 62.3 %all-gather.20.cloned.1.call-start = ((), (), s32[]{:S(2)}) async-start(), calls=%async_computation.7 | async-start | bytes 1572864 | tf_op jit(solution)/shard_map/all_gather | solution.py:111
  7.3 73.6 %all-gather.12.cloned.1.call-start = ((), (), s32[]{:S(2)}) async-start(), calls=%async_computation.2 | async-start | bytes 2621440 | tf_op jit(solution)/shard_map/all_gather | solution.py:124
  8.0 62.5 %copy-start.20 = (f32[2048]{0:T(1024)S(1)}, f32[2048]{0:T(1024)}, u32[]{:S(2)}) copy-start(f32[2048]{0:T(1024)} %param.19) | copy-start | bytes 24580
  8.1 119.6 %all-gather.16.cloned.1.call-start = ((), (), s32[]{:S(2)}) async-start(), calls=%async_computation.4 | async-start | bytes 2621440 | tf_op jit(solution)/shard_map/all_gather | solution.py:123
  8.8 164.8 %all-gather.14.cloned.1.call-start = ((), (), s32[]{:S(2)}) async-start(), calls=%async_computation.3 | async-start | bytes 2621440 | tf_op jit(solution)/shard_map/all_gather | solution.py:125
  9.4 210.1 %all-gather.18.cloned.1.call-start = ((), (), s32[]{:S(2)}) async-start(), calls=%async_computation.5 | async-start | bytes 2621440 | tf_op jit(solution)/shard_map/all_gather | solution.py:126
  10.0 238.9 %all-gather.22.cloned.1.call-start = ((), (), s32[]{:S(2)}) async-start(), calls=%async_computation.8 | async-start | bytes 1310720 | tf_op jit(solution)/shard_map/all_gather | solution.py:18
  68.9 12.1 %copy-start.5 = (bf16[1,256,2048]{2,1,0:T(8,128)(2,1)S(1)}, bf16[1,256,2048]{2,1,0:T(8,128)(2,1)}, u32[]{:S(2)}) copy-start(bf16[1,256,2048]{2,1,0:T(8,128)(2,1)} %all-gather.20.cloned.1.call-done) | copy-start | bytes 3145732
  70.5 103.1 %copy-start.18 = (f32[256]{0:T(256)}, f32[256]{0:T(256)S(1)}, u32[]{:S(2)}) copy-start(f32[256]{0:T(256)S(1)} %add_rsqrt_fusion.1) | copy-start | bytes 3076
  72.2 11.0 %copy-start.10 = (bf16[256,128]{1,0:T(8,128)(2,1)}, bf16[256,128]{1,0:T(8,128)(2,1)S(1)}, u32[]{:S(2)}) copy-start(bf16[256,128]{1,0:T(8,128)(2,1)S(1)} %convolution_convert_fusion.5) | copy-start | bytes 196612
  72.9 118.2 %collective-permute-start.1 = (bf16[128,128]{1,0:T(8,128)(2,1)}, bf16[128,128]{1,0:T(8,128)(2,1)}, u32[]{:S(2)}, u32[]{:S(2)}) collective-permute-start(bf16[128,128]{1,0:T(8,128)(2,1)} %slice.64), channel_id=1, source_target_pairs={{0,8},{8,16},{16,24},{1,9},{9,17},{17,25},{2,10},{10,18},{18,26},{... | collective-permute-start | bytes 98312 | tf_op jit(solution)/shard_map/ppermute | solution.py:41
  176.6 1.3 copy-start.8
  178.0 0.7 copy-start.3
  178.1 0.8 copy-start.1
  178.8 7.6 %copy-start.19 = (f32[256]{0:T(256)S(1)}, f32[256]{0:T(256)}, u32[]{:S(2)}) copy-start(f32[256]{0:T(256)} %copy-done.18) | copy-start | bytes 3076
  178.8 7.6 %copy-start.21 = (f32[2048]{0:T(1024)S(1)}, f32[2048]{0:T(1024)}, u32[]{:S(2)}) copy-start(f32[2048]{0:T(1024)} %param.19) | copy-start | bytes 24580
  185.6 2.7 copy-start.11
  186.4 104.1 %all-gather.24.cloned.1.call-start = ((), (), s32[]{:S(2)}) async-start(), calls=%async_computation.9 | async-start | bytes 2621440 | tf_op jit(solution)/shard_map/all_gather | solution.py:209
  188.3 31.2 %copy-start.6 = (bf16[1,256,2048]{2,1,0:T(8,128)(2,1)S(1)}, bf16[1,256,2048]{2,1,0:T(8,128)(2,1)}, u32[]{:S(2)}) copy-start(bf16[1,256,2048]{2,1,0:T(8,128)(2,1)} %all-gather.20.cloned.1.call-done) | copy-start | bytes 3145732
  188.6 4.3 %collective-permute-start = (bf16[128,128]{1,0:T(8,128)(2,1)S(1)}, bf16[128,128]{1,0:T(8,128)(2,1)S(1)}, u32[]{:S(2)}, u32[]{:S(2)}) collective-permute-start(bf16[128,128]{1,0:T(8,128)(2,1)S(1)} %slice.63), channel_id=1, source_target_pairs={{0,8},{8,16},{16,24},{1,9},{9,17},{17,25},{2,10},{10,18},{18,26},{... | collective-permute-start | bytes 98312 | tf_op jit(solution)/shard_map/ppermute | solution.py:41
  194.9 27.2 %copy-start.14 = (pred[2,128,256]{1,2,0:T(8,128)(4,1)S(1)}, pred[2,128,256]{1,2,0:T(8,128)(4,1)}, u32[]{:S(2)}) copy-start(pred[2,128,256]{1,2,0:T(8,128)(4,1)} %broadcast_and_fusion) | copy-start | bytes 196612
  221.8 1.0 copy-start.17
  248.9 4.6 %copy-start.2 = (f32[256,2,128]{2,0,1:T(8,128)S(1)}, f32[256,2,128]{2,0,1:T(8,128)}, u32[]{:S(2)}) copy-start(f32[256,2,128]{2,0,1:T(8,128)} %copy-done.1) | copy-start | bytes 786436
  248.9 4.6 %copy-start.4 = (f32[256,2,128]{2,0,1:T(8,128)S(1)}, f32[256,2,128]{2,0,1:T(8,128)}, u32[]{:S(2)}) copy-start(f32[256,2,128]{2,0,1:T(8,128)} %copy-done.3) | copy-start | bytes 786436
  248.9 4.6 %copy-start.9 = (f32[1,2,256,256]{3,2,1,0:T(8,128)S(1)}, f32[1,2,256,256]{3,2,1,0:T(8,128)}, u32[]{:S(2)}) copy-start(f32[1,2,256,256]{3,2,1,0:T(8,128)} %param.27) | copy-start | bytes 1572868
  253.5 1.3 copy-start.16
  255.9 65.2 %reduce-scatter.2.cloned.1.call-start = ((), (), s32[]{:S(2)}) async-start(), calls=%async_computation.6 | async-start | bytes 1572864 | tf_op jit(solution)/shard_map/reduce_scatter | solution.py:218
  293.3 1.0 copy-start.7
Sparse Core Ops, SparseCore 0:
  8.9 11.7 all-gather.19
  22.3 58.6 all-gather.11
  82.5 45.0 all-gather.15
  129.1 44.4 all-gather.13
  175.0 44.4 all-gather.17
  220.9 27.9 all-gather.21
  256.0 34.4 all-gather.23
  313.2 7.8 reduce-scatter.1
where the time goes:
time: 331 us; the launch traced here: 330 us
  waiting for transfers between devices  188 us (57%)
  blocking collectives  69.8 us (21%)
  matrix products  23 us (7%)
  local copies, waits for them, and re-layouts  16.4 us (5%)
  between operations  14.8 us (4%)
  other arithmetic  12.8 us (4%)
  starting transfers between devices  5.19 us (2%)
    all_gather x1, waiting for transfers between devices, shards(): lax.all_gather(weights[0], 'sp', axis=0, tiled=True)  44 us
    all_gather x1, waiting for transfers between devices, shards(): lax.all_gather(weights[2], 'sp', axis=0, tiled=True)  42.1 us
    all_gather x1, waiting for transfers between devices, shards(): piece = lax.all_gather(joined, 'fs', axis=0, tiled=True)  34.5 us
    all_gather x1, waiting for transfers between devices, carried_in(): lax.all_gather(part.astype(kind), axis)  25.1 us
    all_gather x1, waiting for transfers between devices, shards(): lax.all_gather(weights[3], 'sp', axis=0, tiled=True)  24.5 us
    all_gather x1, blocking collectives, shards(): lax.all_gather(weights[5], 'sp', axis=0, tiled=True)  21.2 us
    all_gather x1, blocking collectives, shards(): lax.all_gather(weights[4], 'sp', axis=0, tiled=True)  18.4 us
    all_to_all x1, blocking collectives, shards(): lax.all_to_all(partial_rows, 'fs', split_axis=0, concat_axis=2, tiled=True)  16.7 us
  transfers between devices with their start and end apart: 10, of which 8 were waited for; matrix products, arithmetic and copies ran while one was open for 11% of the time, Pallas kernels for 0%

commit v1 on v0

--- a/solution.py
+++ b/solution.py
@@ -108,6 +108,25 @@
     ret_out,
     att_out,
 ):
+
+    def view_spread(target, where_dim, array_axis=2):
+        known, prior = (jax.lax.axis_size("fs"), jax.lax.axis_index("fs"))
+        val = target.shape[where_dim] // known
+        x_new = jnp.roll(target, -prior * val, axis=where_dim)
+        store = [lax.slice_in_dim(x_new, 0, val, axis=where_dim)]
+        for p in range(1, known):
+            state_now = lax.slice_in_dim(x_new, p * val, (p + 1) * val, axis=where_dim)
+            store.append(
+                jax.lax.ppermute(
+                    state_now, "fs", [(nth, (nth + p) % known) for nth in range(known)]
+                )
+            )
+        return jnp.roll(
+            jnp.concatenate(store[::-1], axis=array_axis),
+            shift=(prior + 1) * store[0].shape[array_axis],
+            axis=array_axis,
+        )
+
     gathered = lax.all_gather(tokens[0], "tp", axis=1, tiled=True)
     row_count = gathered.shape[0]
     as_float = gathered.astype(jnp.float32)
@@ -214,7 +233,7 @@
         "srh,hd->srd", piece[:, :, ret_width:], att_out, preferred_element_type=jnp.float32
     )
     partial_rows = product.astype(jnp.bfloat16)
-    regrouped = lax.all_to_all(partial_rows, "fs", split_axis=0, concat_axis=2, tiled=True)
+    regrouped = view_spread(partial_rows, 0)
     mixed = lax.psum_scatter(
         regrouped[0].astype(jnp.float32).astype(jnp.bfloat16), "tp", scatter_dimension=1, tiled=True
     )

time: 331 us -> 328 us (level)
  blocking collectives: 69.8 us -> 53 us
  waiting for transfers between devices: 188 us -> 200 us
  starting transfers between devices: 5.19 us -> 8.77 us
    all_to_all x1 -> x0, blocking collectives: 16.7 us -> none  [shards(): lax.all_to_all(partial_rows, 'fs', split_axis=0, concat_axis=2, tiled=True)]
    ppermute x0 -> x3, waiting for transfers between devices: none -> 11.2 us  [view_spread(): jax.lax.ppermute(state_now, 'fs', [(nth, (nth + p) % known) for nth in ra...]
    ppermute x0 -> x3, starting transfers between devices: none -> 3.54 us  [view_spread(): jax.lax.ppermute(state_now, 'fs', [(nth, (nth + p) % known) for nth in ra...]
  transfers between devices with their start and end apart: 10 -> 13, of which waited for: 8 -> 10; matrix products, arithmetic and copies ran while one was open for 11% -> 11% of each run, Pallas kernels for 0% -> 0%
where the time goes in v1:
time: 328 us; the launch traced here: 327 us
  waiting for transfers between devices  200 us (61%)
  blocking collectives  53 us (16%)
  matrix products  22.9 us (7%)
  between operations  14.8 us (5%)
  local copies, waits for them, and re-layouts  14.4 us (4%)
  other arithmetic  13.2 us (4%)
  starting transfers between devices  8.77 us (3%)
    all_gather x1, waiting for transfers between devices, shards(): lax.all_gather(weights[0], 'sp', axis=0, tiled=True)  44 us
    all_gather x1, waiting for transfers between devices, shards(): lax.all_gather(weights[2], 'sp', axis=0, tiled=True)  42.1 us
    all_gather x1, waiting for transfers between devices, shards(): piece = lax.all_gather(joined, 'fs', axis=0, tiled=True)  34.5 us
    all_gather x1, waiting for transfers between devices, carried_in(): lax.all_gather(part.astype(kind), axis)  25.1 us
    all_gather x1, waiting for transfers between devices, shards(): lax.all_gather(weights[3], 'sp', axis=0, tiled=True)  24.6 us
    all_gather x1, blocking collectives, shards(): lax.all_gather(weights[5], 'sp', axis=0, tiled=True)  21.1 us
    all_gather x1, blocking collectives, shards(): lax.all_gather(weights[4], 'sp', axis=0, tiled=True)  18.3 us
    dot_general x6, matrix products, shards(): jnp.dot(normed, piece, preferred_element_type=jnp.float32)  13.6 us
  transfers between devices with their start and end apart: 13, of which 10 were waited for; matrix products, arithmetic and copies ran while one was open for 11% of the time, Pallas kernels for 0%

profile of v1, /device:TPU:0, one launch (start us, length us, event | category | flops | bytes accessed | tf_op | source)
XLA Modules:
  0.0 326.9 jit_solution(15120475782086089852)
XLA Ops:
  7.3 0.7 all-gather.12.cloned.1.call-update
  12.8 13.6 %all-reduce = bf16[8]{0:T(256)(128)(2,1)S(1)} all-reduce(bf16[8]{0:T(256)(128)(2,1)S(1)} %dynamic-update-slice), channel_id=3, replica_groups=mesh['sp'=4,'fs'=4,'tp'=2] {'sp'}, use_global_device_ids=true, to_apply=%add | all-reduce | flops 8 | bytes 32
  26.5 18.3 %all_gather.42 = bf16[2048,128]{1,0:T(8,128)(2,1)S(1)} all-gather(bf16[512,128]{1,0:T(8,128)(2,1)S(1)} %copy-done.12), channel_id=1, replica_groups=mesh['sp'=4,'fs'=4,'tp'=2] {'sp'}, dimensions={0}, use_global_device_ids=true | all-gather | bytes 655360 | tf_op jit(solution)/shard_map/all_gather | solution.py:146
  45.6 21.1 %all_gather.41 = bf16[2048,128]{1,0:T(8,128)(2,1)} all-gather(bf16[512,128]{1,0:T(8,128)(2,1)S(1)} %copy-done.13), channel_id=1, replica_groups=mesh['sp'=4,'fs'=4,'tp'=2] {'sp'}, dimensions={0}, use_global_device_ids=true | all-gather | bytes 655360 | tf_op jit(solution)/shard_map/all_gather | solution.py:147
  66.7 1.2 multiply_cosine_fusion
  67.9 0.8 broadcast_and_fusion
  68.7 1.6 fusion.25
  70.3 1.7 convolution_convert_fusion.5
  72.7 2.7 collective-permute-start.1
  75.4 5.5 %all-gather.12.cloned.1.call-done = bf16[2048,512]{1,0:T(8,128)(2,1)} async-done(((bf16[512,512]{1,0:T(8,128)(2,1)}), bf16[2048,512]{1,0:T(8,128)(2,1)}) %all-gather.12.cloned.1.call-update) | async-done | bytes 2097168 | tf_op jit(solution)/shard_map/all_gather | solution.py:143
  80.8 2.3 fusion.31
  83.5 44.0 %all-gather.16.cloned.1.call-done = bf16[2048,512]{1,0:T(8,128)(2,1)} async-done(((bf16[512,512]{1,0:T(8,128)(2,1)}), bf16[2048,512]{1,0:T(8,128)(2,1)}) %all-gather.16.cloned.1.call-update) | async-done | bytes 2097168 | tf_op jit(solution)/shard_map/all_gather | solution.py:142
  127.5 2.7 fusion.33
  130.2 1.1 reshape.298
  131.4 42.1 %all-gather.14.cloned.1.call-done = bf16[2048,512]{1,0:T(8,128)(2,1)} async-done(((bf16[512,512]{1,0:T(8,128)(2,1)}), bf16[2048,512]{1,0:T(8,128)(2,1)}) %all-gather.14.cloned.1.call-update) | async-done | bytes 2097168 | tf_op jit(solution)/shard_map/all_gather | solution.py:144
  173.5 2.7 fusion.32
  176.5 1.3 fusion.67
  178.8 6.7 %while.29 = (s32[]{:T(128)}, f32[2,256,256]{2,1,0:T(8,128)S(1)}, f32[2,2,128,256]{3,2,1,0:T(8,128)}, f32[2,2,128]{2,1,0:T(2,128)S(1)}, f32[2,2,128,256]{3,2,0,1:...) while((s32[]{:T(128)}, f32[2,256,256]{2,1,0:T(8,128)S(1)}, ...), condition=%wide.region_3.4_spmd.clone, body=%wide.region_1.3_spmd.clone.sunk | while | flops 604880896 | bytes 4242084 | solution.py:167
  180.1 1.2 fusion.97
  181.3 0.8 convolution_add_fusion.3
  183.5 1.2 fusion.97
  184.7 0.8 convolution_add_fusion.3
  185.5 0.7 convert_element_type.102
  186.3 1.9 convolution_convert_fusion.6
  188.6 2.2 collective-permute-start
  190.9 0.8 pad_maximum_fusion.2
  191.9 1.0 collective-permute-done
  193.1 1.3 copy.63
  194.8 24.6 %all-gather.18.cloned.1.call-done = bf16[2048,512]{1,0:T(8,128)(2,1)} async-done(((bf16[512,512]{1,0:T(8,128)(2,1)}), bf16[2048,512]{1,0:T(8,128)(2,1)}) %all-gather.18.cloned.1.call-update) | async-done | bytes 2097168 | tf_op jit(solution)/shard_map/all_gather | solution.py:145
  219.4 2.3 convolution_convert_fusion.1
  223.7 25.1 %all-gather.22.cloned.1.call-done = bf16[8,256,256]{2,1,0:T(8,128)(2,1)} async-done(((bf16[2,256,256]{2,1,0:T(8,128)(2,1)}), bf16[8,256,256]{2,1,0:T(8,128)(2,1)}) %all-gather.22.cloned.1.call-update) | async-done | bytes 1048592 | tf_op jit(solution)/shard_map/all_gather | solution.py:18
  248.8 4.6 %while.30 = (s32[]{:T(128)}, f32[2]{0:T(128)S(1)}, f32[2,256,256]{2,1,0:T(8,128)S(1)}, s32[]{:T(128)}, bf16[4,2]{1,0:T(4,128)(2,1)S(1)}, /*index=5*/bf16[4,2,256,256]{3,2,1,0:T(8,128)(2,1)}, s32[]{:T(128)}, s32[]{:T(128)}) while((s32[]{:T(128)}, f32[2]{0:T(128)S(1)}, f32[2,256,256]{2,1,0:T(8,128)S(1)}, s32[]{:T(128)}, ...), condition=%wide.region_7.8_spmd.clone, body=%wide.region_6.7_spmd.clone.sunk | while | flops 655372 | bytes 1310871 | solution.py:35
  248.8 1.2 fusion.98
  250.0 1.1 fusion.98
  251.2 1.1 fusion.98
  252.3 1.1 fusion.98
  253.5 1.2 fusion.69
  254.9 0.8 pad_maximum_fusion.1
  255.9 34.5 %all-gather.24.cloned.1.call-done = bf16[1024,1024]{0,1:T(8,128)(2,1)} async-done(((bf16[256,1024]{0,1:T(8,128)(2,1)}), bf16[1024,1024]{0,1:T(8,128)(2,1)}) %all-gather.24.cloned.1.call-update) | async-done | bytes 2097168 | tf_op jit(solution)/shard_map/all_gather | solution.py:228
  290.4 2.9 copy.79
  293.2 0.7 fusion.37
  294.3 0.7 add_convert_fusion
  295.5 1.5 collective-permute-start.2
  297.0 1.5 collective-permute-start.3
  299.0 5.7 %collective-permute-done.2 = bf16[1,256,512]{2,1,0:T(8,128)(2,1)S(1)} collective-permute-done((bf16[1,256,512]{2,1,0:T(8,128)(2,1)S(1)}, bf16[1,256,512]{2,1,0:T(8,128)(2,1)S(1)}, u32[]{:S(2)}, u32[]{:S(2)}) %collective-permute-start.2) | collective-permute-done | bytes 262176 | tf_op jit(solution)/shard_map/ppermute | solution.py:120
  304.7 5.5 %collective-permute-done.3 = bf16[1,256,512]{2,1,0:T(8,128)(2,1)S(1)} collective-permute-done((bf16[1,256,512]{2,1,0:T(8,128)(2,1)S(1)}, bf16[1,256,512]{2,1,0:T(8,128)(2,1)S(1)}, u32[]{:S(2)}, u32[]{:S(2)}) %collective-permute-start.3) | collective-permute-done | bytes 262176 | tf_op jit(solution)/shard_map/ppermute | solution.py:120
  310.5 1.1 dynamic-slice_bitcast_fusion
  311.6 8.5 %reduce-scatter.2.cloned.1.call-done = bf16[256,1024]{1,0:T(8,128)(2,1)} async-done(((bf16[256,2048]{1,0:T(8,128)(2,1)}), bf16[256,1024]{1,0:T(8,128)(2,1)}) %reduce-scatter.2.cloned.1.call-update) | async-done | bytes 524304 | tf_op jit(solution)/shard_map/reduce_scatter | solution.py:237
  (152 shorter events, 15.8 us)
Async XLA Ops:
  6.5 286.7 %copy-start = (bf16[512,512]{1,0:T(8,128)(2,1)S(1)}, bf16[512,512]{1,0:T(8,128)(2,1)}, u32[]{:S(2)}) copy-start(bf16[512,512]{1,0:T(8,128)(2,1)} %param.30) | copy-start | bytes 1572868
  6.5 4.8 %copy-start.23 = (u32[32]{0:T(128)S(1)}, u32[32]{0:T(128)}, u32[]{:S(2)}) copy-start(u32[32]{0:T(128)} %constant.141) | copy-start | bytes 388
  6.5 3.5 %copy-start.15 = (f32[1,2,256]{2,1,0:T(2,128)S(1)}, f32[1,2,256]{2,1,0:T(2,128)}, u32[]{:S(2)}) copy-start(f32[1,2,256]{2,1,0:T(2,128)} %param.26) | copy-start | bytes 6148
  6.5 20.0 %copy-start.12 = (bf16[512,128]{1,0:T(8,128)(2,1)S(1)}, bf16[512,128]{1,0:T(8,128)(2,1)}, u32[]{:S(2)}) copy-start(bf16[512,128]{1,0:T(8,128)(2,1)} %param.24) | copy-start | bytes 393220
  6.5 38.4 %copy-start.22 = (f32[8]{0:T(128)S(1)}, f32[8]{0:T(128)}, u32[]{:S(2)}) copy-start(f32[8]{0:T(128)} %param.29) | copy-start | bytes 100
  6.5 39.1 %copy-start.13 = (bf16[512,128]{1,0:T(8,128)(2,1)S(1)}, bf16[512,128]{1,0:T(8,128)(2,1)}, u32[]{:S(2)}) copy-start(bf16[512,128]{1,0:T(8,128)(2,1)} %param.25) | copy-start | bytes 393220
  6.6 62.1 %all-gather.20.cloned.1.call-start = ((), (), s32[]{:S(2)}) async-start(), calls=%async_computation.6 | async-start | bytes 1572864 | tf_op jit(solution)/shard_map/all_gather | solution.py:130
  7.3 73.5 %all-gather.12.cloned.1.call-start = ((), (), s32[]{:S(2)}) async-start(), calls=%async_computation.1 | async-start | bytes 2621440 | tf_op jit(solution)/shard_map/all_gather | solution.py:143
  8.0 62.3 %copy-start.20 = (f32[2048]{0:T(1024)S(1)}, f32[2048]{0:T(1024)}, u32[]{:S(2)}) copy-start(f32[2048]{0:T(1024)} %param.19) | copy-start | bytes 24580
  8.1 119.5 %all-gather.16.cloned.1.call-start = ((), (), s32[]{:S(2)}) async-start(), calls=%async_computation.3 | async-start | bytes 2621440 | tf_op jit(solution)/shard_map/all_gather | solution.py:142
  8.8 164.7 %all-gather.14.cloned.1.call-start = ((), (), s32[]{:S(2)}) async-start(), calls=%async_computation.2 | async-start | bytes 2621440 | tf_op jit(solution)/shard_map/all_gather | solution.py:144
  9.4 210.0 %all-gather.18.cloned.1.call-start = ((), (), s32[]{:S(2)}) async-start(), calls=%async_computation.4 | async-start | bytes 2621440 | tf_op jit(solution)/shard_map/all_gather | solution.py:145
  10.0 238.8 %all-gather.22.cloned.1.call-start = ((), (), s32[]{:S(2)}) async-start(), calls=%async_computation.7 | async-start | bytes 1310720 | tf_op jit(solution)/shard_map/all_gather | solution.py:18
  68.7 12.1 %copy-start.5 = (bf16[1,256,2048]{2,1,0:T(8,128)(2,1)S(1)}, bf16[1,256,2048]{2,1,0:T(8,128)(2,1)}, u32[]{:S(2)}) copy-start(bf16[1,256,2048]{2,1,0:T(8,128)(2,1)} %all-gather.20.cloned.1.call-done) | copy-start | bytes 3145732
  70.3 103.1 %copy-start.18 = (f32[256]{0:T(256)}, f32[256]{0:T(256)S(1)}, u32[]{:S(2)}) copy-start(f32[256]{0:T(256)S(1)} %add_rsqrt_fusion.1) | copy-start | bytes 3076
  72.0 11.1 %copy-start.10 = (bf16[256,128]{1,0:T(8,128)(2,1)}, bf16[256,128]{1,0:T(8,128)(2,1)S(1)}, u32[]{:S(2)}) copy-start(bf16[256,128]{1,0:T(8,128)(2,1)S(1)} %convolution_convert_fusion.5) | copy-start | bytes 196612
  72.7 118.2 %collective-permute-start.1 = (bf16[128,128]{1,0:T(8,128)(2,1)}, bf16[128,128]{1,0:T(8,128)(2,1)}, u32[]{:S(2)}, u32[]{:S(2)}) collective-permute-start(bf16[128,128]{1,0:T(8,128)(2,1)} %slice.80), channel_id=1, source_target_pairs={{0,8},{8,16},{16,24},{1,9},{9,17},{17,25},{2,10},{10,18},{18,26},{... | collective-permute-start | bytes 98312 | tf_op jit(solution)/shard_map/ppermute | solution.py:41
  176.5 1.3 copy-start.8
  177.9 0.7 copy-start.3
  178.0 0.8 copy-start.1
  178.7 7.6 %copy-start.19 = (f32[256]{0:T(256)S(1)}, f32[256]{0:T(256)}, u32[]{:S(2)}) copy-start(f32[256]{0:T(256)} %copy-done.18) | copy-start | bytes 3076
  178.7 7.6 %copy-start.21 = (f32[2048]{0:T(1024)S(1)}, f32[2048]{0:T(1024)}, u32[]{:S(2)}) copy-start(f32[2048]{0:T(1024)} %param.19) | copy-start | bytes 24580
  185.5 2.7 copy-start.11
  186.3 104.1 %all-gather.24.cloned.1.call-start = ((), (), s32[]{:S(2)}) async-start(), calls=%async_computation.8 | async-start | bytes 2621440 | tf_op jit(solution)/shard_map/all_gather | solution.py:228
  188.2 31.2 %copy-start.6 = (bf16[1,256,2048]{2,1,0:T(8,128)(2,1)S(1)}, bf16[1,256,2048]{2,1,0:T(8,128)(2,1)}, u32[]{:S(2)}) copy-start(bf16[1,256,2048]{2,1,0:T(8,128)(2,1)} %all-gather.20.cloned.1.call-done) | copy-start | bytes 3145732
  188.6 4.3 %collective-permute-start = (bf16[128,128]{1,0:T(8,128)(2,1)S(1)}, bf16[128,128]{1,0:T(8,128)(2,1)S(1)}, u32[]{:S(2)}, u32[]{:S(2)}) collective-permute-start(bf16[128,128]{1,0:T(8,128)(2,1)S(1)} %slice.79), channel_id=1, source_target_pairs={{0,8},{8,16},{16,24},{1,9},{9,17},{17,25},{2,10},{10,18},{18,26},{... | collective-permute-start | bytes 98312 | tf_op jit(solution)/shard_map/ppermute | solution.py:41
  194.8 27.2 %copy-start.14 = (pred[2,128,256]{1,2,0:T(8,128)(4,1)S(1)}, pred[2,128,256]{1,2,0:T(8,128)(4,1)}, u32[]{:S(2)}) copy-start(pred[2,128,256]{1,2,0:T(8,128)(4,1)} %broadcast_and_fusion) | copy-start | bytes 196612
  221.7 1.0 copy-start.17
  248.8 4.6 %copy-start.2 = (f32[256,2,128]{2,0,1:T(8,128)S(1)}, f32[256,2,128]{2,0,1:T(8,128)}, u32[]{:S(2)}) copy-start(f32[256,2,128]{2,0,1:T(8,128)} %copy-done.1) | copy-start | bytes 786436
  248.8 4.6 %copy-start.4 = (f32[256,2,128]{2,0,1:T(8,128)S(1)}, f32[256,2,128]{2,0,1:T(8,128)}, u32[]{:S(2)}) copy-start(f32[256,2,128]{2,0,1:T(8,128)} %copy-done.3) | copy-start | bytes 786436
  248.8 4.6 %copy-start.9 = (f32[1,2,256,256]{3,2,1,0:T(8,128)S(1)}, f32[1,2,256,256]{3,2,1,0:T(8,128)}, u32[]{:S(2)}) copy-start(f32[1,2,256,256]{3,2,1,0:T(8,128)} %param.27) | copy-start | bytes 1572868
  253.5 1.3 copy-start.16
  255.8 64.3 %reduce-scatter.2.cloned.1.call-start = ((), (), s32[]{:S(2)}) async-start(), calls=%async_computation.5 | async-start | bytes 1572864 | tf_op jit(solution)/shard_map/reduce_scatter | solution.py:237
  293.2 1.0 copy-start.7
  295.5 9.2 %collective-permute-start.2 = (bf16[1,256,512]{2,1,0:T(8,128)(2,1)S(1)}, bf16[1,256,512]{2,1,0:T(8,128)(2,1)S(1)}, u32[]{:S(2)}, u32[]{:S(2)}) collective-permute-start(bf16[1,256,512]{2,1,0:T(8,128)(2,1)S(1)} %get-tuple-element.248), channel_id=1, source_target_pairs={{0,6},{2,0},{4,2},{6,4},{1,7},{3,1},{5,3},{7,5},{8,14},{10,8},{12,... | collective-permute-start | bytes 786440 | tf_op jit(solution)/shard_map/ppermute | solution.py:120
  297.0 13.2 %collective-permute-start.3 = (bf16[1,256,512]{2,1,0:T(8,128)(2,1)S(1)}, bf16[1,256,512]{2,1,0:T(8,128)(2,1)S(1)}, u32[]{:S(2)}, u32[]{:S(2)}) collective-permute-start(bf16[1,256,512]{2,1,0:T(8,128)(2,1)S(1)} %get-tuple-element.247), channel_id=1, source_target_pairs={{0,4},{2,6},{4,0},{6,2},{1,5},{3,7},{5,1},{7,3},{8,12},{10,14},{12... | collective-permute-start | bytes 786440 | tf_op jit(solution)/shard_map/ppermute | solution.py:120
  298.4 11.8 %collective-permute-start.4 = (bf16[1,256,512]{2,1,0:T(8,128)(2,1)S(1)}, bf16[1,256,512]{2,1,0:T(8,128)(2,1)S(1)}, u32[]{:S(2)}, u32[]{:S(2)}) collective-permute-start(bf16[1,256,512]{2,1,0:T(8,128)(2,1)S(1)} %get-tuple-element.246), channel_id=1, source_target_pairs={{0,2},{2,4},{4,6},{6,0},{1,3},{3,5},{5,7},{7,1},{8,10},{10,12},{12... | collective-permute-start | bytes 786440 | tf_op jit(solution)/shard_map/ppermute | solution.py:120
Sparse Core Ops, SparseCore 0:
  8.9 11.7 all-gather.19
  22.3 58.5 all-gather.11
  82.4 45.0 all-gather.15
  129.0 44.4 all-gather.13
  174.9 44.4 all-gather.17
  220.8 27.9 all-gather.21
  255.9 34.4 all-gather.23
  311.7 8.3 reduce-scatter.1
